TPU v7x, 32 devices: a whole 2x2x4 slice. The times are simulated.
32 devices in a mesh: sp: 16 (over z, y, core), tp: 2 (over x).
Axes of the slice: x: 2, y: 2, z: 4, core: 2. Of those that a mesh axis runs over, the one named last changes fastest.
Arguments:
- queries: bfloat16 [16384, 1024], P('sp', 'tp'), may hold values from -8 to 8
- keyvals: bfloat16 [16384, 8, 128], P('sp', 'tp'), may hold values from -8 to 8
- head_sink_logit: float32 [16], P('tp'), may hold values from 2 to 7
- doc_ids: int32 [16384], P('sp'), may hold values from 0 to 7, never falling along the last dimension, each value on 1 to 4096 neighbouring positions
- stream_in: bfloat16 [16384, 2048], P(('sp', 'tp')), may hold values from -6 to 6
- out_weight: bfloat16 [1024, 2048], replicated, may hold values from -1.5 to 1.5
- first_gain: float32 [2048], replicated, may hold values from 0.1 to 1.9
- up_weight: bfloat16 [2048, 8192], P('sp', 'tp'), may hold values from -0.125 to 0.125
- down_weight: bfloat16 [8192, 2048], P('tp', 'sp'), may hold values from -0.0625 to 0.0625
- second_gain: float32 [2048], replicated, may hold values from 0.1 to 1.9
Outputs:
- layer_out: bfloat16 [16384, 2048], P(('sp', 'tp'))
Inputs may be any that keep to these rules, and one draw needn't show every extreme that they name: `doc_ids`: document numbers never fall along the sequence.
All inputs are finite; a program needn't handle non-finite values.
Results may differ from a plain program's by a relative error of at most 0.013.
Values may be sent and summed in bfloat16 or wider, within the bound.
A program may use at most 128 MiB of HBM per device.

v0:
```python
import jax
import jax.numpy as jnp
from jax import lax
from jax.sharding import PartitionSpec as P

HEAD_SIZE = 64
WINDOW_REACH = 128


NEG_LARGE = -1e30
NORM_EPS = 1e-05


def padded(block, sides, width):
    for axis, dim in sides:
        count = lax.axis_size(axis)
        forward = [(i, i + 1) for i in range(count - 1)]
        backward = [(target, source) for source, target in forward]
        low = lax.ppermute(
            lax.slice_in_dim(block, block.shape[dim] - width, None, axis=dim), axis, forward
        )
        high = lax.ppermute(lax.slice_in_dim(block, 0, width, axis=dim), axis, backward)
        block = jnp.concatenate([low, block, high], axis=dim)
    return block


def layer_norm(stream, gain_row):
    centre = jnp.mean(stream, axis=-1, keepdims=True)
    shifted = stream - centre
    spread = jnp.mean(shifted * shifted, axis=-1, keepdims=True)
    return shifted * lax.rsqrt(spread + NORM_EPS) * gain_row


def attend(queries, keyvals, head_sink_logit, doc_ids):
    tok_rows = queries.shape[0]
    kv_heads = keyvals.shape[1]
    heads_per_group = queries.shape[1] // (HEAD_SIZE * kv_heads)
    block_list = tok_rows // WINDOW_REACH
    score_scale = HEAD_SIZE ** (-0.5)
    doc_marks = doc_ids.astype(jnp.bfloat16)
    rim_keys, rim_docs = (
        padded(keyvals, (("sp", 0),), WINDOW_REACH),
        padded(doc_marks, (("sp", 0),), WINDOW_REACH),
    )
    padded_rows = rim_keys.reshape(block_list + 2, WINDOW_REACH, kv_heads, 2 * HEAD_SIZE)
    banded = jnp.concatenate([padded_rows[:-2], padded_rows[1:-1], padded_rows[2:]], axis=1)
    doc_ext = rim_docs.reshape(block_list + 2, WINDOW_REACH)
    doc_band = jnp.concatenate([doc_ext[:-2], doc_ext[1:-1], doc_ext[2:]], axis=1)
    offset = lax.axis_index("sp") * tok_rows
    total_rows = tok_rows * lax.axis_size("sp")
    query_pos = offset + jnp.arange(tok_rows, dtype=jnp.int32).reshape(block_list, WINDOW_REACH, 1)
    key_pos = (
        offset
        + (
            jnp.arange(block_list, dtype=jnp.int32)[:, None] * WINDOW_REACH
            + jnp.arange(3 * WINDOW_REACH, dtype=jnp.int32)[None, :]
            - WINDOW_REACH
        )[:, None, :]
    )
    allowed = (
        (jnp.abs(query_pos - key_pos) <= WINDOW_REACH)
        & (key_pos >= 0)
        & (key_pos < total_rows)
        & (doc_marks.reshape(block_list, WINDOW_REACH, 1) == doc_band[:, None, :])
    )
    query_block_list = queries.reshape(
        block_list, WINDOW_REACH, kv_heads, heads_per_group, HEAD_SIZE
    )
    scores = (
        jnp.einsum(
            "nqhgd,nkhd->nhgqk",
            query_block_list,
            banded[..., :HEAD_SIZE],
            preferred_element_type=jnp.float32,
        )
        * score_scale
    )
    scores = jnp.where(allowed[:, None, None], scores, NEG_LARGE)
    sink_col = head_sink_logit.reshape(kv_heads, heads_per_group)[None, :, :, None, None]
    highest = jnp.maximum(jnp.max(scores, axis=-1, keepdims=True), sink_col)
    powers = jnp.exp(scores - highest)
    denominator = jnp.sum(powers, axis=-1, keepdims=True) + jnp.exp(sink_col - highest)
    weights = (powers / denominator).astype(jnp.bfloat16)
    mixed_out = jnp.einsum(
        "nhgqk,nkhd->nqhgd", weights, banded[..., HEAD_SIZE:], preferred_element_type=jnp.float32
    )
    return mixed_out.astype(jnp.bfloat16).reshape(tok_rows, kv_heads * heads_per_group * HEAD_SIZE)


def per_device(
    queries,
    keyvals,
    head_sink_logit,
    doc_ids,
    stream_in,
    out_weight,
    first_gain,
    up_weight,
    down_weight,
    second_gain,
):
    up_whole = lax.all_gather(up_weight, "sp", axis=0, tiled=True)
    down_whole = lax.all_gather(down_weight, "sp", axis=1, tiled=True)
    attended = attend(queries, keyvals, head_sink_logit, doc_ids)
    tp_count = lax.axis_size("tp")
    own_rows = attended.shape[0] // tp_count
    by_peer = attended.reshape(tp_count, own_rows, attended.shape[1])
    projected = jnp.dot(
        lax.all_to_all(by_peer, "tp", split_axis=0, concat_axis=2, tiled=True)[0],
        out_weight,
        preferred_element_type=jnp.float32,
    )[None][0]
    first_stream = layer_norm(stream_in.astype(jnp.float32) + projected, first_gain).astype(
        jnp.bfloat16
    )
    hidden = jnp.dot(
        lax.all_gather(first_stream, "tp", axis=0, tiled=True),
        up_whole,
        preferred_element_type=jnp.float32,
    )
    active = jnp.square(jnp.maximum(hidden, 0.0)).astype(jnp.bfloat16)
    mixed_out = lax.psum_scatter(
        jnp.dot(active, down_whole, preferred_element_type=jnp.float32).astype(jnp.bfloat16),
        "tp",
        scatter_dimension=0,
        tiled=True,
    ).astype(jnp.float32)
    return layer_norm(first_stream.astype(jnp.float32) + mixed_out, second_gain).astype(
        jnp.bfloat16
    )


def solution(mesh):
    return jax.shard_map(
        per_device,
        mesh=mesh,
        in_specs=(
            P("sp", "tp"),
            P("sp", "tp", None),
            P("tp"),
            P("sp"),
            P(("sp", "tp"), None),
            P(),
            P(),
            P("sp", "tp"),
            P("tp", "sp"),
            P(),
        ),
        out_specs=P(("sp", "tp"), None),
        check_vma=False,
    )
```

profile of v0, /device:TPU:0, one launch (start us, length us, event | category | flops | bytes accessed | tf_op | source)
XLA Modules:
  0.0 477.8 jit_solution(12057201046544516895)
XLA Ops:
  6.5 0.8 convert_element_type.34
  7.3 2.4 collective-permute-start.2
  9.7 1.3 collective-permute-start.3
  11.0 1.4 copy.26
  12.4 5.8 %collective-permute-start = (bf16[128,4,128]{2,0,1:T(8,128)(2,1)S(1)}, bf16[128,4,128]{2,0,1:T(8,128)(2,1)}, u32[]{:S(2)}, u32[]{:S(2)}) collective-permute-start(bf16[128,4,128]{2,0,1:T(8,128)(2,1)S(1)} %get-tuple-element.7), channel_id=1, source_target_pairs={{0,2},{2,4},{4,6},{6,8},{8,10},{10,12},{12,14},{14,16},{16,18},{18... | collective-permute-start | bytes 393224 | tf_op jit(solution)/shard_map/ppermute | solution.py:19
  18.2 1.3 collective-permute-start.1
  19.5 0.7 convert_bitcast_fusion
  20.2 0.1 fusion.13
  20.3 0.1 add_add_fusion
  20.4 2.3 copy.32
  22.6 2.1 reshape.167
  24.7 0.1 max.24
  24.8 2.3 fusion.9
  27.1 1.3 pad_maximum_fusion.2
  28.4 0.7 copy.31
  29.1 0.7 copy.33
  29.7 1.8 pad_maximum_fusion
  31.6 0.1 copy-done.6
  31.6 2.5 fusion.1
  34.2 0.1 broadcast_maximum_fusion
  34.3 3.4 fusion
  37.7 0.1 exponential_add_fusion
  37.8 3.6 fusion.11
  41.4 0.7 copy.37
  42.1 0.4 reshape_reshape.3
  42.6 0.2 copy.38
  42.8 17.2 %all_to_all.15 = bf16[2,512,512]{1,2,0:T(8,128)(2,1)S(1)} all-to-all(bf16[2,512,512]{1,2,0:T(8,128)(2,1)S(1)} %copy.38), channel_id=1, replica_groups=mesh['sp'=16,'tp'=2] {'tp'}, dimensions={0} | all-to-all | bytes 2097152 | tf_op jit(solution)/shard_map/all_to_all | solution.py:109
  60.0 4.2 fusion.20
  64.2 0.6 multiply_reduce_fusion.1
  64.8 1.4 copy-done
  66.1 1.9 multiply_convert_fusion.2
  68.1 0.0 all-gather.4.cloned.1.call-update
  68.1 0.0 all-gather.6.cloned.1.call-start
  68.1 0.7 all-gather.6.cloned.1.call-update
  68.8 0.0 all-gather.8.cloned.1.call-start
  68.9 0.7 all-gather.8.cloned.1.call-update
  69.6 0.0 reduce-scatter.2.cloned.1.call-start
  69.6 56.9 %all-gather.4.cloned.1.call-done = bf16[1024,2048]{1,0:T(8,128)(2,1)} async-done(((bf16[512,2048]{1,0:T(8,128)(2,1)}), bf16[1024,2048]{1,0:T(8,128)(2,1)}) %all-gather.4.cloned.1.call-update) | async-done | bytes 4194320 | tf_op jit(solution)/shard_map/all_gather | solution.py:117
  126.5 128.6 %all-gather.6.cloned.1.call-done = bf16[2048,4096]{1,0:T(8,128)(2,1)} async-done(((bf16[128,4096]{1,0:T(8,128)(2,1)}), bf16[2048,4096]{1,0:T(8,128)(2,1)}) %all-gather.6.cloned.1.call-update) | async-done | bytes 16777232 | tf_op jit(solution)/shard_map/all_gather | solution.py:102
  255.1 22.9 %fusion.44 = bf16[1024,4096]{1,0:T(8,128)(2,1)} fusion(bf16[2048,4096]{1,0:T(8,128)(2,1)} %all-gather.6.cloned.1.call-done, bf16[1024,2048]{1,0:T(8,128)(2,1)} %all-gather.4.cloned.1.call-done), kind=kOutput, calls=%bitcast_fusion.1.clone.1 | convolution fusion | flops 17192452096 | bytes 29360128 | tf_op jit(solution)/shard_map/dot_general | solution.py:116
  278.0 107.4 %all-gather.8.cloned.1.call-done = bf16[4096,2048]{1,0:T(8,128)(2,1)} async-done(((bf16[4096,128]{1,0:T(8,128)(2,1)}), bf16[4096,2048]{1,0:T(8,128)(2,1)}) %all-gather.8.cloned.1.call-update) | async-done | bytes 16777232 | tf_op jit(solution)/shard_map/all_gather | solution.py:103
  385.4 23.7 %convolution_convert_fusion = bf16[1024,2048]{1,0:T(8,128)(2,1)} fusion(bf16[4096,2048]{1,0:T(8,128)(2,1)} %all-gather.8.cloned.1.call-done, bf16[1024,4096]{1,0:T(8,128)(2,1)} %fusion.44), kind=kOutput, calls=%fused_computation.15 | convolution fusion | flops 17181966336 | bytes 29360128 | tf_op jit(solution)/shard_map/dot_general | solution.py:123
  409.1 52.7 %reduce-scatter.2.cloned.1.call-done = bf16[512,2048]{1,0:T(8,128)(2,1)} async-done(((bf16[1024,2048]{1,0:T(8,128)(2,1)}), bf16[512,2048]{1,0:T(8,128)(2,1)}) %reduce-scatter.2.cloned.1.call-update) | async-done | bytes 2097168 | tf_op jit(solution)/shard_map/reduce_scatter | solution.py:122
  461.8 3.9 fusion.4
  465.8 0.1 copy-done.1
  465.8 0.7 copy-done.2
  466.5 1.2 multiply_reduce_fusion
  467.8 3.5 multiply_convert_fusion.1
  (34 shorter events, 0.1 us)
Async XLA Ops:
  6.5 16.1 %copy-start.7 = (bf16[1024,512]{1,0:T(8,128)(2,1)S(1)}, bf16[1024,512]{1,0:T(8,128)(2,1)}, u32[]{:S(2)}) copy-start(bf16[1024,512]{1,0:T(8,128)(2,1)} %param.10) | copy-start | bytes 3145732
  6.5 18.2 %copy-start.10 = (f32[8]{0:T(128)S(1)}, f32[8]{0:T(128)}, u32[]{:S(2)}) copy-start(f32[8]{0:T(128)} %param.12) | copy-start | bytes 100
  6.5 119.9 %all-gather.4.cloned.1.call-start = ((), (), s32[]{:S(2)}) async-start(), calls=%async_computation.2 | async-start | bytes 6291456 | tf_op jit(solution)/shard_map/all_gather | solution.py:117
  7.3 17.5 %collective-permute-start.2 = (bf16[128]{0:T(256)(128)(2,1)S(1)}, bf16[128]{0:T(256)(128)(2,1)S(1)}, u32[]{:S(2)}, u32[]{:S(2)}) collective-permute-start(bf16[128]{0:T(256)(128)(2,1)S(1)} %get-tuple-element.11), channel_id=1, source_target_pairs={{0,2},{2,4},{4,6},{6,8},{8,10},{10,12},{12,14},{14,16},{16,18},{18... | collective-permute-start | bytes 776 | tf_op jit(solution)/shard_map/ppermute | solution.py:19
  9.7 15.1 %collective-permute-start.3 = (bf16[128]{0:T(256)(128)(2,1)S(1)}, bf16[128]{0:T(256)(128)(2,1)S(1)}, u32[]{:S(2)}, u32[]{:S(2)}) collective-permute-start(bf16[128]{0:T(256)(128)(2,1)S(1)} %get-tuple-element.12), channel_id=1, source_target_pairs={{2,0},{4,2},{6,4},{8,6},{10,8},{12,10},{14,12},{16,14},{18,16},{20... | collective-permute-start | bytes 776 | tf_op jit(solution)/shard_map/ppermute | solution.py:22
  12.4 14.7 %collective-permute-start = (bf16[128,4,128]{2,0,1:T(8,128)(2,1)S(1)}, bf16[128,4,128]{2,0,1:T(8,128)(2,1)}, u32[]{:S(2)}, u32[]{:S(2)}) collective-permute-start(bf16[128,4,128]{2,0,1:T(8,128)(2,1)S(1)} %get-tuple-element.7), channel_id=1, source_target_pairs={{0,2},{2,4},{4,6},{6,8},{8,10},{10,12},{12,14},{14,16},{16,18},{18... | collective-permute-start | bytes 393224 | tf_op jit(solution)/shard_map/ppermute | solution.py:19
  18.2 8.9 %collective-permute-start.1 = (bf16[128,4,128]{2,0,1:T(8,128)(2,1)S(1)}, bf16[128,4,128]{2,0,1:T(8,128)(2,1)}, u32[]{:S(2)}, u32[]{:S(2)}) collective-permute-start(bf16[128,4,128]{2,0,1:T(8,128)(2,1)S(1)} %get-tuple-element.8), channel_id=1, source_target_pairs={{2,0},{4,2},{6,4},{8,6},{10,8},{12,10},{14,12},{16,14},{18,16},{20... | collective-permute-start | bytes 393224 | tf_op jit(solution)/shard_map/ppermute | solution.py:22
  29.7 1.9 copy-start.6
  31.6 2.5 copy-start.4
  34.3 3.6 copy-start.5
  42.6 17.4 %copy-start.3 = (bf16[1024,2048]{1,0:T(8,128)(2,1)S(1)}, bf16[1024,2048]{1,0:T(8,128)(2,1)}, u32[]{:S(2)}) copy-start(bf16[1024,2048]{1,0:T(8,128)(2,1)} %param.15) | copy-start | bytes 12582916
  64.2 1.9 copy-start
  64.2 1.9 copy-start.8
  68.1 187.0 %all-gather.6.cloned.1.call-start = ((), (), s32[]{:S(2)}) async-start(), calls=%async_computation.3 | async-start | bytes 17825792 | tf_op jit(solution)/shard_map/all_gather | solution.py:102
  68.8 316.5 %all-gather.8.cloned.1.call-start = ((), (), s32[]{:S(2)}) async-start(), calls=%async_computation.4 | async-start | bytes 17825792 | tf_op jit(solution)/shard_map/all_gather | solution.py:103
  69.6 392.2 %reduce-scatter.2.cloned.1.call-start = ((), (), s32[]{:S(2)}) async-start(), calls=%async_computation.5 | async-start | bytes 6291456 | tf_op jit(solution)/shard_map/reduce_scatter | solution.py:122
  461.8 4.0 copy-start.1
  461.8 4.7 copy-start.2
  465.7 2.0 copy-start.9
Sparse Core Ops, SparseCore 0:
  68.2 58.2 all-gather.3
  128.6 126.4 all-gather.5
  257.3 128.0 all-gather.7
  409.2 52.5 reduce-scatter.1
where the time goes:
time: 478 us
  waiting for transfers between devices  347 us (73%)
  matrix products  56.9 us (12%)
  other arithmetic  21.8 us (5%)
  blocking collectives  17.2 us (4%)
  between operations  13.4 us (3%)
  starting transfers between devices  10.9 us (2%)
  local copies, waits for them, and re-layouts  10.6 us (2%)
    all_gather x1, waiting for transfers between devices, per_device(): up_whole = lax.all_gather(up_weight, 'sp', axis=0, tiled=True)  129 us
    all_gather x1, waiting for transfers between devices, per_device(): down_whole = lax.all_gather(down_weight, 'sp', axis=1, tiled=True)  107 us
    all_gather x1, waiting for transfers between devices, per_device(): lax.all_gather(first_stream, 'tp', axis=0, tiled=True)  56.9 us
    reduce_scatter x1, waiting for transfers between devices, per_device(): lax.psum_scatter(jnp.dot(active, down_whole, preferred_element_type=jnp.f...  52.7 us
    dot_general x1, matrix products, per_device(): jnp.dot(active, down_whole, preferred_element_type=jnp.float32)  23.7 us
    dot_general x1, matrix products, per_device(): jnp.dot(lax.all_gather(first_stream, 'tp', axis=0, tiled=True), up_whole,...  22.9 us
    all_to_all x1, blocking collectives, per_device(): lax.all_to_all(by_peer, 'tp', split_axis=0, concat_axis=2, tiled=True)[0]  17.2 us
  transfers between devices with their start and end apart: 8, of which 4 were waited for; matrix products, arithmetic and copies ran while one was open for 7% of the time, Pallas kernels for 0%

commit v1 on v0

--- a/solution.py
+++ b/solution.py
@@ -1,6 +1,7 @@
 import jax
 import jax.numpy as jnp
 from jax import lax
+from jax.experimental import pallas as pl
 from jax.sharding import PartitionSpec as P
 
 HEAD_SIZE = 64
@@ -87,6 +88,39 @@
     return mixed_out.astype(jnp.bfloat16).reshape(tok_rows, kv_heads * heads_per_group * HEAD_SIZE)
 
 
+def cyclic(block, axis, shift):
+    count = lax.axis_size(axis)
+    return lax.ppermute(block, axis, [(i, (i + shift) % count) for i in range(count)])
+
+
+def gather_columns(block, axis):
+    count = lax.axis_size(axis)
+    line_count = count // 4
+    me = lax.axis_index(axis)
+    line, side = me // 4, me % 2
+    rows, width = block.shape
+
+    def along(shift):
+        return [(i, (i + 4 * shift) % count) for i in range(count)]
+
+    across = [(i, i ^ 2) for i in range(count)]
+    beside = [(i, i ^ 1) for i in range(count)]
+    this_row = [block] + [lax.ppermute(block, axis, along(shift)) for shift in range(1, line_count)]
+    other_row = [lax.ppermute(block, axis, across)]
+    other_row += [lax.ppermute(piece, axis, across) for piece in this_row[1:]]
+
+    row = (me // 2) % 2
+    whole = jnp.zeros((rows, count * width), block.dtype)
+    for pieces, from_row in ((this_row, row), (other_row, 1 - row)):
+        for shift, piece in enumerate(pieces):
+            source = lax.rem(line - shift + line_count, line_count)
+            partner = lax.ppermute(piece, axis, beside)
+            first = 4 * source + 2 * from_row
+            whole = lax.dynamic_update_slice(whole, piece, (0, (first + side) * width))
+            whole = lax.dynamic_update_slice(whole, partner, (0, (first + 1 - side) * width))
+    return whole
+
+
 def per_device(
     queries,
     keyvals,
@@ -100,7 +134,9 @@
     second_gain,
 ):
     up_whole = lax.all_gather(up_weight, "sp", axis=0, tiled=True)
-    down_whole = lax.all_gather(down_weight, "sp", axis=1, tiled=True)
+    cut = down_weight.shape[0] // 2
+    down_low = lax.all_gather(down_weight[:cut], "sp", axis=1, tiled=True)
+    down_high = gather_columns(down_weight[cut:], "sp")
     attended = attend(queries, keyvals, head_sink_logit, doc_ids)
     tp_count = lax.axis_size("tp")
     own_rows = attended.shape[0] // tp_count
@@ -109,25 +145,53 @@
         lax.all_to_all(by_peer, "tp", split_axis=0, concat_axis=2, tiled=True)[0],
         out_weight,
         preferred_element_type=jnp.float32,
-    )[None][0]
+    )
     first_stream = layer_norm(stream_in.astype(jnp.float32) + projected, first_gain).astype(
         jnp.bfloat16
     )
-    hidden = jnp.dot(
-        lax.all_gather(first_stream, "tp", axis=0, tiled=True),
-        up_whole,
-        preferred_element_type=jnp.float32,
-    )
-    active = jnp.square(jnp.maximum(hidden, 0.0)).astype(jnp.bfloat16)
-    mixed_out = lax.psum_scatter(
-        jnp.dot(active, down_whole, preferred_element_type=jnp.float32).astype(jnp.bfloat16),
-        "tp",
-        scatter_dimension=0,
-        tiled=True,
-    ).astype(jnp.float32)
-    return layer_norm(first_stream.astype(jnp.float32) + mixed_out, second_gain).astype(
-        jnp.bfloat16
-    )
+
+    def activate(rows):
+        hidden = jnp.dot(rows, up_whole, preferred_element_type=jnp.float32)
+        return lax.optimization_barrier(jnp.square(jnp.maximum(hidden, 0.0)).astype(jnp.bfloat16))
+
+    def contract(active):
+        early = lax.optimization_barrier(
+            jnp.dot(active[:, cut:], down_high, preferred_element_type=jnp.float32)
+        )
+        late = jnp.dot(active[:, :cut], down_low, preferred_element_type=jnp.float32)
+        return lax.optimization_barrier((early + late).astype(jnp.bfloat16))
+
+    visiting = [cyclic(first_stream, "tp", shift) for shift in range(1, tp_count)]
+    own_active = activate(first_stream)
+    visiting_active = [activate(rows) for rows in visiting]
+    visiting_parts = [contract(active) for active in visiting_active]
+    returned = [cyclic(part, "tp", -shift) for shift, part in enumerate(visiting_parts, 1)]
+    own_part = contract(own_active)
+    return closing_norm(first_stream, second_gain, [own_part] + returned)
+
+
+def closing_kernel(stream_ref, gain_ref, *refs):
+    mixed = refs[0][...].astype(jnp.float32)
+    for partial_ref in refs[1:-1]:
+        mixed = mixed + partial_ref[...].astype(jnp.float32)
+    refs[-1][...] = layer_norm(
+        stream_ref[...].astype(jnp.float32) + mixed, gain_ref[...]
+    ).astype(refs[-1].dtype)
+
+
+def closing_norm(stream, gain, partials):
+    rows, width = stream.shape
+    tile = min(128, rows)
+    row_spec = pl.BlockSpec((tile, width), lambda i: (i, 0))
+    return pl.pallas_call(
+        closing_kernel,
+        grid=(rows // tile,),
+        out_shape=jax.ShapeDtypeStruct(stream.shape, stream.dtype),
+        in_specs=[row_spec, pl.BlockSpec((1, width), lambda i: (0, 0))]
+        + [row_spec] * len(partials),
+        out_specs=row_spec,
+        name="closing_norm",
+    )(stream, gain.reshape(1, width), *partials)
 
 
 def solution(mesh):

time: 478 us -> 346 us (0.72)
  waiting for transfers between devices: 347 us -> 115 us
  starting transfers between devices: 10.9 us -> 93.3 us
  local copies, waits for them, and re-layouts: 10.6 us -> 37.5 us
  blocking collectives: 17.2 us -> 0 us
  matrix products: 56.9 us -> 65.8 us
  other arithmetic: 21.8 us -> 14.3 us
  Pallas kernels: 0 us -> 5.52 us
    all_gather x1, waiting for transfers between devices: 129 us -> 0.01 us  [per_device(): up_whole = lax.all_gather(up_weight, 'sp', axis=0, tiled=True)]
    all_gather x2 -> x1, waiting for transfers between devices: 164 us -> 44.3 us  [per_device(): down_low = lax.all_gather(down_weight[:cut], 'sp', axis=1, tiled=True)]
    ppermute x0 -> x17, starting transfers between devices: none -> 81 us  [the longest x3 37.4 us: gather_columns(): lax.ppermute(block, axis, along(shift))]
    ppermute x0 -> x17, waiting for transfers between devices: none -> 69.9 us  [the longest x2 34.8 us: cyclic(): lax.ppermute(block, axis, [(i, (i + shift) % count) for i in range(count)])]
    reduce_scatter x1 -> x0, waiting for transfers between devices: 52.7 us -> none  [per_device(): lax.psum_scatter(jnp.dot(active, down_whole, preferred_element_type=jnp.f...]
    dynamic_update_slice x0 -> x15, local copies, waits for them, and re-layouts: none -> 19.9 us  [the longest x8 10.4 us: gather_columns(): lax.dynamic_update_slice(whole, partner, (0, (first + 1 - side) * width))]
    all_to_all x1 -> x0, blocking collectives: 17.2 us -> none  [per_device(): lax.all_to_all(by_peer, 'tp', split_axis=0, concat_axis=2, tiled=True)[0]]
    dot_general x2 -> x6, matrix products: 46.6 us -> 54.2 us  [the longest x2 25.5 us: activate(): hidden = jnp.dot(rows, up_whole, preferred_element_type=jnp.float32)]
  transfers between devices with their start and end apart: 8 -> 24, of which waited for: 4 -> 7; matrix products, arithmetic and copies ran while one was open for 7% -> 31% of each run, Pallas kernels for 0% -> 0%
where the time goes in v1:
time: 346 us; the launch traced here: 345 us
  waiting for transfers between devices  115 us (33%)
  starting transfers between devices  93.3 us (27%)
  matrix products  65.8 us (19%)
  local copies, waits for them, and re-layouts  37.5 us (11%)
  other arithmetic  14.3 us (4%)
  between operations  13.9 us (4%)
  Pallas kernels  5.52 us (2%)
    all_gather x1, waiting for transfers between devices, per_device(): down_low = lax.all_gather(down_weight[:cut], 'sp', axis=1, tiled=True)  44.3 us
    ppermute x3, starting transfers between devices, gather_columns(): lax.ppermute(block, axis, along(shift))  37.4 us
    ppermute x2, waiting for transfers between devices, cyclic(): lax.ppermute(block, axis, [(i, (i + shift) % count) for i in range(count)])  34.8 us
    dot_general x2, matrix products, activate(): hidden = jnp.dot(rows, up_whole, preferred_element_type=jnp.float32)  25.5 us
    ppermute x3, starting transfers between devices, gather_columns(): other_row += [lax.ppermute(piece, axis, across) for piece in this_row[1:]]  22 us
    ppermute x3, waiting for transfers between devices, gather_columns(): lax.ppermute(block, axis, along(shift))  19.3 us
    ppermute x8, starting transfers between devices, gather_columns(): partner = lax.ppermute(piece, axis, beside)  18.6 us
    dot_general x2, matrix products, contract(): jnp.dot(active[:, cut:], down_high, preferred_element_type=jnp.float32)  16.5 us
  transfers between devices with their start and end apart: 24, of which 7 were waited for; matrix products, arithmetic and copies ran while one was open for 31% of the time, Pallas kernels for 0%

profile of v1, /device:TPU:0, one launch (start us, length us, event | category | flops | bytes accessed | tf_op | source)
XLA Modules:
  0.0 345.4 jit_solution(1278108086606163455)
XLA Ops:
  7.4 4.3 %broadcast_in_dim.16 = bf16[2048,2048]{1,0:T(8,128)(2,1)} broadcast(bf16[]{:T(256)} %constant.87.clone.1), dimensions={} | broadcast | bytes 8388610 | tf_op jit(solution)/shard_map/broadcast_in_dim | solution.py:113
  11.7 1.3 fusion.24
  13.5 2.6 collective-permute-start.5
  16.1 2.5 collective-permute-start.7
  18.7 1.9 collective-permute-start.2
  20.6 1.3 collective-permute-start.3
  24.1 1.4 copy.32
  25.5 2.1 reshape.158
  28.2 4.3 %collective-permute-start = (bf16[128,4,128]{2,0,1:T(8,128)(2,1)}, bf16[128,4,128]{2,0,1:T(8,128)(2,1)S(1)}, u32[]{:S(2)}, u32[]{:S(2)}) collective-permute-start(bf16[128,4,128]{2,0,1:T(8,128)(2,1)} %get-tuple-element.10), channel_id=1, source_target_pairs={{0,2},{2,4},{4,6},{6,8},{8,10},{10,12},{12,14},{14,16},{16,18},{18... | collective-permute-start | bytes 393224 | tf_op jit(solution)/shard_map/ppermute | solution.py:20
  32.5 1.3 collective-permute-start.1
  33.8 3.1 fusion.15
  38.8 1.8 pad_maximum_fusion
  40.7 2.5 fusion.1
  43.4 3.4 fusion
  46.9 3.6 %fusion.17 = bf16[8,128,4,2,64]{1,4,3,2,0:T(8,128)(2,1)S(1)} fusion(f32[8,4,384,128,2]{3,2,4,1,0:T(8,128)S(1)} %get-tuple-element.19, f32[8,4,2,128]{3,2,1,0:T(2,128)S(1)} %exponential_add_fusion, f32[8,4,2,128]{3,2,1,0:T(2,128)S(1)} %broadcast_maximum_fusion, pred[8,128,384]{1,2,0:T(8,128)(4,1)S(1)} %fusion.15, bf16[8,384,4,128]{1,3,2,0:T(8,128)(2,1)S(1)} %copy-done.4), kind=kOutput, calls=%fused_computation.31 | convolution fusion | flops 418906112 | bytes 15663104 | tf_op jit(solution)/shard_map/nhgqk,nkhd->nqhgd/dot_general | solution.py:85
  51.7 1.1 copy.38
  52.8 3.6 %all-to-all-start = ((bf16[2,512,512]{1,2,0:T(8,128)(2,1)}), bf16[2,512,512]{1,2,0:T(8,128)(2,1)S(1)}, u32[]{:S(2)}, u32[]{:S(2)}) async-start(bf16[2,512,512]{1,2,0:T(8,128)(2,1)} %copy.38), calls=%async_computation | async-start | bytes 2097152 | tf_op jit(solution)/shard_map/all_to_all | solution.py:145
  56.4 32.3 %collective-permute-start.9 = (bf16[2048,128]{1,0:T(8,128)(2,1)}, bf16[2048,128]{1,0:T(8,128)(2,1)S(1)}, u32[]{:S(2)}, u32[]{:S(2)}) collective-permute-start(bf16[2048,128]{1,0:T(8,128)(2,1)} %get-tuple-element.7), channel_id=1, source_target_pairs={{0,24},{2,26},{4,28},{6,30},{8,0},{10,2},{12,4},{14,6},{16,8},{18,... | collective-permute-start | bytes 1572872 | tf_op jit(solution)/shard_map/ppermute | solution.py:108
  88.7 5.1 %collective-permute-start.6 = (bf16[2048,128]{1,0:T(8,128)(2,1)}, bf16[2048,128]{1,0:T(8,128)(2,1)}, u32[]{:S(2)}, u32[]{:S(2)}) collective-permute-start(bf16[2048,128]{1,0:T(8,128)(2,1)} %collective-permute-done.5), channel_id=1, source_target_pairs={{0,2},{2,0},{4,6},{6,4},{8,10},{10,8},{12,14},{14,12},{16,18},{18,... | collective-permute-start | bytes 1572872 | tf_op jit(solution)/shard_map/ppermute | solution.py:117
  94.3 2.0 constant_dynamic-update-slice_fusion.14
  96.3 1.9 constant_dynamic-update-slice_fusion.13
  98.3 5.5 %fusion.27 = (f32[512]{0:T(512)S(1)}, f32[512,2048]{1,0:T(8,128)S(1)}) fusion(bf16[512,1024]{0,1:T(8,128)(2,1)S(1)} %bitcast.60, bf16[1024,2048]{1,0:T(8,128)(2,1)} %param.15, bf16[512,2048]{1,0:T(8,128)(2,1)} %param.14), kind=kOutput, calls=%fused_computation.69 | convolution fusion | flops 2150628864 | bytes 11536384 | tf_op jit(solution)/shard_map/dot_general | solution.py:144
  104.9 19.3 %collective-permute-done.9 = bf16[2048,128]{1,0:T(8,128)(2,1)S(1)} collective-permute-done((bf16[2048,128]{1,0:T(8,128)(2,1)}, bf16[2048,128]{1,0:T(8,128)(2,1)S(1)}, u32[]{:S(2)}, u32[]{:S(2)}) %collective-permute-start.9) | collective-permute-done | bytes 524320 | tf_op jit(solution)/shard_map/ppermute | solution.py:108
  124.3 21.2 %collective-permute-start.15 = (bf16[2048,128]{1,0:T(8,128)(2,1)}, bf16[2048,128]{1,0:T(8,128)(2,1)S(1)}, u32[]{:S(2)}, u32[]{:S(2)}) collective-permute-start(bf16[2048,128]{1,0:T(8,128)(2,1)} %collective-permute-done.7), channel_id=1, source_target_pairs={{0,4},{2,6},{4,0},{6,2},{8,12},{10,14},{12,8},{14,10},{16,20},{18,... | collective-permute-start | bytes 1572872 | tf_op jit(solution)/shard_map/ppermute | solution.py:110
  145.4 5.7 %collective-permute-start.10 = (bf16[2048,128]{1,0:T(8,128)(2,1)S(1)}, bf16[2048,128]{1,0:T(8,128)(2,1)S(1)}, u32[]{:S(2)}, u32[]{:S(2)}) collective-permute-start(bf16[2048,128]{1,0:T(8,128)(2,1)S(1)} %collective-permute-done.9), channel_id=1, source_target_pairs={{0,2},{2,0},{4,6},{6,4},{8,10},{10,8},{12,14},{14,12},{16,18},{18,... | collective-permute-start | bytes 1572872 | tf_op jit(solution)/shard_map/ppermute | solution.py:117
  151.2 2.0 constant_dynamic-update-slice_fusion.12
  153.4 1.9 constant_dynamic-update-slice_fusion.11
  155.4 1.9 constant_dynamic-update-slice_fusion.10
  158.2 1.5 collective-permute-start.19
  159.9 8.1 %collective-permute-done.15 = bf16[2048,128]{1,0:T(8,128)(2,1)S(1)} collective-permute-done((bf16[2048,128]{1,0:T(8,128)(2,1)}, bf16[2048,128]{1,0:T(8,128)(2,1)S(1)}, u32[]{:S(2)}, u32[]{:S(2)}) %collective-permute-start.15) | collective-permute-done | bytes 524320 | tf_op jit(solution)/shard_map/ppermute | solution.py:110
  168.0 5.0 %collective-permute-start.16 = (bf16[2048,128]{1,0:T(8,128)(2,1)S(1)}, bf16[2048,128]{1,0:T(8,128)(2,1)S(1)}, u32[]{:S(2)}, u32[]{:S(2)}) collective-permute-start(bf16[2048,128]{1,0:T(8,128)(2,1)S(1)} %collective-permute-done.15), channel_id=1, source_target_pairs={{0,2},{2,0},{4,6},{6,4},{8,10},{10,8},{12,14},{14,12},{16,18},{18,... | collective-permute-start | bytes 1572872 | tf_op jit(solution)/shard_map/ppermute | solution.py:117
  173.1 7.5 %collective-permute-done.17 = bf16[2048,128]{1,0:T(8,128)(2,1)S(1)} collective-permute-done((bf16[2048,128]{1,0:T(8,128)(2,1)S(1)}, bf16[2048,128]{1,0:T(8,128)(2,1)S(1)}, u32[]{:S(2)}, u32[]{:S(2)}) %collective-permute-start.17) | collective-permute-done | bytes 524320 | tf_op jit(solution)/shard_map/ppermute | solution.py:110
  180.6 2.0 collective-permute-start.18
  185.3 2.0 constant_dynamic-update-slice_fusion.5
  191.8 14.5 %collective-permute-done.19 = bf16[512,2048]{1,0:T(8,128)(2,1)} collective-permute-done((bf16[512,2048]{1,0:T(8,128)(2,1)S(1)}, bf16[512,2048]{1,0:T(8,128)(2,1)}, u32[]{:S(2)}, u32[]{:S(2)}) %collective-permute-start.19) | collective-permute-done | bytes 2097184 | tf_op jit(solution)/shard_map/ppermute | solution.py:93
  206.3 13.1 %multiply_convert_fusion = bf16[512,4096]{1,0:T(8,128)(2,1)S(1)} fusion(bf16[512,2048]{1,0:T(8,128)(2,1)} %collective-permute-done.19, bf16[2048,4096]{1,0:T(8,128)(2,1)} %all-gather.3.cloned.1.call-done), kind=kOutput, calls=%fused_computation.5 | convolution fusion | flops 8596226048 | bytes 23068672 | tf_op jit(solution)/shard_map/dot_general | solution.py:154
  219.4 2.0 copy-done.13
  221.4 9.4 %fusion.5 = f32[512,2048]{1,0:T(8,128)} fusion(bf16[2048,2048]{1,0:T(8,128)(2,1)} %constant_dynamic-update-slice_fusion, bf16[512,4096]{1,0:T(8,128)(2,1)S(1)} %multiply_convert_fusion), kind=kOutput, calls=%fused_computation.16 | convolution fusion | flops 4294967296 | bytes 14680064 | tf_op jit(solution)/shard_map/dot_general | solution.py:159
  230.8 44.3 %all-gather.5.cloned.1.call-done = bf16[2048,2048]{1,0:T(8,128)(2,1)} async-done(((bf16[2048,128]{1,0:T(8,128)(2,1)}), bf16[2048,2048]{1,0:T(8,128)(2,1)}) %all-gather.5.cloned.1.call-update) | async-done | bytes 8388624 | tf_op jit(solution)/shard_map/all_gather | solution.py:138
  275.2 7.7 %fusion.3 = f32[512,2048]{1,0:T(8,128)S(1)} fusion(bf16[2048,2048]{1,0:T(8,128)(2,1)} %all-gather.5.cloned.1.call-done, bf16[512,4096]{1,0:T(8,128)(2,1)} %copy-done.13), kind=kOutput, calls=%fused_computation.14 | convolution fusion | flops 4294967296 | bytes 14680064 | tf_op jit(solution)/shard_map/dot_general | solution.py:161
  283.9 1.5 collective-permute-start.20
  285.4 12.4 %multiply_convert_fusion.1 = bf16[512,4096]{1,0:T(8,128)(2,1)S(1)} fusion(bf16[512,2048]{1,0:T(8,128)(2,1)S(1)} %multiply_convert_fusion.2.stream_ref, bf16[2048,4096]{1,0:T(8,128)(2,1)} %all-gather.3.cloned.1.call-done), kind=kOutput, calls=%fused_computation.6 | convolution fusion | flops 8596226048 | bytes 23068672 | tf_op jit(solution)/shard_map/dot_general | solution.py:154
  297.9 7.1 %fusion.9 = f32[512,2048]{1,0:T(8,128)S(1)} fusion(bf16[2048,2048]{1,0:T(8,128)(2,1)} %constant_dynamic-update-slice_fusion, bf16[512,4096]{1,0:T(8,128)(2,1)S(1)} %multiply_convert_fusion.1), kind=kOutput, calls=%fused_computation.20 | convolution fusion | flops 4294967296 | bytes 14680064 | tf_op jit(solution)/shard_map/dot_general | solution.py:159
  305.0 4.5 %fusion.7 = f32[512,2048]{1,0:T(8,128)S(1)} fusion(bf16[2048,2048]{1,0:T(8,128)(2,1)S(1)} %bitcast.66, bf16[512,4096]{1,0:T(8,128)(2,1)S(1)} %multiply_convert_fusion.1), kind=kOutput, calls=%fused_computation.18 | convolution fusion | flops 4294967296 | bytes 14680064 | tf_op jit(solution)/shard_map/dot_general | solution.py:161
  309.5 1.9 add_convert_fusion.1.refs_0_
  311.4 20.3 %collective-permute-done.20.refs_1_ = bf16[512,2048]{1,0:T(8,128)(2,1)S(1)} collective-permute-done((bf16[512,2048]{1,0:T(8,128)(2,1)S(1)}, bf16[512,2048]{1,0:T(8,128)(2,1)S(1)}, u32[]{:S(2)}, u32[]{:S(2)}) %collective-permute-start.20) | collective-permute-done | bytes 2097184 | tf_op jit(solution)/shard_map/ppermute | solution.py:93
  331.8 1.3 copy-done.5
  333.1 5.5 %closing_norm.1 = bf16[512,2048]{1,0:T(8,128)(2,1)} custom-call(bf16[512,2048]{1,0:T(8,128)(2,1)} %copy-done, f32[1,2048]{1,0:T(1,128)} %bitcast.64, bf16[512,2048]{1,0:T(8,128)(2,1)} %add_convert_fusion.1.refs_0_, bf16[512,2048]{1,0:T(8,128)(2,1)} %copy-done.5), custom_call_target="tpu_custom_call" | custom-call | tf_op jit(solution)/shard_map/closing_norm/pallas_call | solution.py:186
  (93 shorter events, 18.8 us)
Async XLA Ops:
  6.5 5.2 %copy-start.8 = (bf16[4096,128]{1,0:T(8,128)(2,1)S(1)}, bf16[4096,128]{1,0:T(8,128)(2,1)}, u32[]{:S(2)}) copy-start(bf16[4096,128]{1,0:T(8,128)(2,1)} %param.18) | copy-start | bytes 3145732
  6.5 12.2 %copy-start.10 = (s32[1024]{0:T(1024)S(1)}, s32[1024]{0:T(1024)}, u32[]{:S(2)}) copy-start(s32[1024]{0:T(1024)} %param.13) | copy-start | bytes 12292
  6.5 15.4 %copy-start.2 = (bf16[1024,4,128]{2,1,0:T(4,128)(2,1)S(1)}, bf16[1024,4,128]{2,1,0:T(4,128)(2,1)}, u32[]{:S(2)}) copy-start(bf16[1024,4,128]{2,1,0:T(4,128)(2,1)} %param.11) | copy-start | bytes 3145732
  6.5 199.8 %all-gather.3.cloned.1.call-start = ((), (), s32[]{:S(2)}) async-start(), calls=%async_computation.1 | async-start | bytes 17825792 | tf_op jit(solution)/shard_map/all_gather | solution.py:136
  7.3 267.9 %all-gather.5.cloned.1.call-start = ((), (), s32[]{:S(2)}) async-start(), calls=%async_computation.2 | async-start | bytes 8912896 | tf_op jit(solution)/shard_map/all_gather | solution.py:138
  7.4 18.1 %copy-start.7 = (bf16[1024,512]{1,0:T(8,128)(2,1)S(1)}, bf16[1024,512]{1,0:T(8,128)(2,1)}, u32[]{:S(2)}) copy-start(bf16[1024,512]{1,0:T(8,128)(2,1)} %param.10) | copy-start | bytes 3145732
  11.7 15.8 %copy-start.12 = (f32[8]{0:T(128)S(1)}, f32[8]{0:T(128)}, u32[]{:S(2)}) copy-start(f32[8]{0:T(128)} %param.12) | copy-start | bytes 100
  13.0 80.8 %collective-permute-start.4 = (bf16[2048,128]{1,0:T(8,128)(2,1)}, bf16[2048,128]{1,0:T(8,128)(2,1)}, u32[]{:S(2)}, u32[]{:S(2)}) collective-permute-start(bf16[2048,128]{1,0:T(8,128)(2,1)} %get-tuple-element.7), channel_id=1, source_target_pairs={{0,2},{2,0},{4,6},{6,4},{8,10},{10,8},{12,14},{14,12},{16,18},{18,... | collective-permute-start | bytes 1572872 | tf_op jit(solution)/shard_map/ppermute | solution.py:117
  13.5 75.2 %collective-permute-start.5 = (bf16[2048,128]{1,0:T(8,128)(2,1)}, bf16[2048,128]{1,0:T(8,128)(2,1)}, u32[]{:S(2)}, u32[]{:S(2)}) collective-permute-start(bf16[2048,128]{1,0:T(8,128)(2,1)} %get-tuple-element.7), channel_id=1, source_target_pairs={{0,8},{2,10},{4,12},{6,14},{8,16},{10,18},{12,20},{14,22},{16,24},... | collective-permute-start | bytes 1572872 | tf_op jit(solution)/shard_map/ppermute | solution.py:108
  16.1 78.2 %collective-permute-start.7 = (bf16[2048,128]{1,0:T(8,128)(2,1)}, bf16[2048,128]{1,0:T(8,128)(2,1)}, u32[]{:S(2)}, u32[]{:S(2)}) collective-permute-start(bf16[2048,128]{1,0:T(8,128)(2,1)} %get-tuple-element.7), channel_id=1, source_target_pairs={{0,16},{2,18},{4,20},{6,22},{8,24},{10,26},{12,28},{14,30},{16,0},... | collective-permute-start | bytes 1572872 | tf_op jit(solution)/shard_map/ppermute | solution.py:108
  18.7 9.5 %collective-permute-start.2 = (bf16[128]{0:T(256)(128)(2,1)S(1)}, bf16[128]{0:T(256)(128)(2,1)S(1)}, u32[]{:S(2)}, u32[]{:S(2)}) collective-permute-start(bf16[128]{0:T(256)(128)(2,1)S(1)} %get-tuple-element.14), channel_id=1, source_target_pairs={{0,2},{2,4},{4,6},{6,8},{8,10},{10,12},{12,14},{14,16},{16,18},{18... | collective-permute-start | bytes 776 | tf_op jit(solution)/shard_map/ppermute | solution.py:20
  20.6 11.9 %collective-permute-start.3 = (bf16[128]{0:T(256)(128)(2,1)S(1)}, bf16[128]{0:T(256)(128)(2,1)S(1)}, u32[]{:S(2)}, u32[]{:S(2)}) collective-permute-start(bf16[128]{0:T(256)(128)(2,1)S(1)} %get-tuple-element.15), channel_id=1, source_target_pairs={{2,0},{4,2},{6,4},{8,6},{10,8},{12,10},{14,12},{16,14},{18,16},{20... | collective-permute-start | bytes 776 | tf_op jit(solution)/shard_map/ppermute | solution.py:23
  28.2 8.7 %collective-permute-start = (bf16[128,4,128]{2,0,1:T(8,128)(2,1)}, bf16[128,4,128]{2,0,1:T(8,128)(2,1)S(1)}, u32[]{:S(2)}, u32[]{:S(2)}) collective-permute-start(bf16[128,4,128]{2,0,1:T(8,128)(2,1)} %get-tuple-element.10), channel_id=1, source_target_pairs={{0,2},{2,4},{4,6},{6,8},{8,10},{10,12},{12,14},{14,16},{16,18},{18... | collective-permute-start | bytes 393224 | tf_op jit(solution)/shard_map/ppermute | solution.py:20
  32.5 4.7 %collective-permute-start.1 = (bf16[128,4,128]{2,0,1:T(8,128)(2,1)}, bf16[128,4,128]{2,0,1:T(8,128)(2,1)S(1)}, u32[]{:S(2)}, u32[]{:S(2)}) collective-permute-start(bf16[128,4,128]{2,0,1:T(8,128)(2,1)} %get-tuple-element.11), channel_id=1, source_target_pairs={{2,0},{4,2},{6,4},{8,6},{10,8},{12,10},{14,12},{16,14},{18,16},{20... | collective-permute-start | bytes 393224 | tf_op jit(solution)/shard_map/ppermute | solution.py:23
  38.8 1.9 copy-start.6
  40.7 2.5 copy-start.3
  40.7 2.5 copy-start.9
  43.4 3.6 %copy-start.4 = (bf16[8,384,4,128]{1,3,2,0:T(8,128)(2,1)S(1)}, bf16[8,384,4,128]{1,3,2,0:T(8,128)(2,1)}, u32[]{:S(2)}) copy-start(bf16[8,384,4,128]{1,3,2,0:T(8,128)(2,1)} %copy-done.3) | copy-start | bytes 9437188
  52.8 45.5 %all-to-all-start = ((bf16[2,512,512]{1,2,0:T(8,128)(2,1)}), bf16[2,512,512]{1,2,0:T(8,128)(2,1)S(1)}, u32[]{:S(2)}, u32[]{:S(2)}) async-start(bf16[2,512,512]{1,2,0:T(8,128)(2,1)} %copy.38), calls=%async_computation | async-start | bytes 2097152 | tf_op jit(solution)/shard_map/all_to_all | solution.py:145
  56.4 67.9 %collective-permute-start.9 = (bf16[2048,128]{1,0:T(8,128)(2,1)}, bf16[2048,128]{1,0:T(8,128)(2,1)S(1)}, u32[]{:S(2)}, u32[]{:S(2)}) collective-permute-start(bf16[2048,128]{1,0:T(8,128)(2,1)} %get-tuple-element.7), channel_id=1, source_target_pairs={{0,24},{2,26},{4,28},{6,30},{8,0},{10,2},{12,4},{14,6},{16,8},{18,... | collective-permute-start | bytes 1572872 | tf_op jit(solution)/shard_map/ppermute | solution.py:108
  88.7 64.4 %collective-permute-start.11 = (bf16[2048,128]{1,0:T(8,128)(2,1)}, bf16[2048,128]{1,0:T(8,128)(2,1)S(1)}, u32[]{:S(2)}, u32[]{:S(2)}) collective-permute-start(bf16[2048,128]{1,0:T(8,128)(2,1)} %get-tuple-element.7), channel_id=1, source_target_pairs={{0,4},{2,6},{4,0},{6,2},{8,12},{10,14},{12,8},{14,10},{16,20},{18,... | collective-permute-start | bytes 1572872 | tf_op jit(solution)/shard_map/ppermute | solution.py:109
  88.7 56.7 %collective-permute-start.6 = (bf16[2048,128]{1,0:T(8,128)(2,1)}, bf16[2048,128]{1,0:T(8,128)(2,1)}, u32[]{:S(2)}, u32[]{:S(2)}) collective-permute-start(bf16[2048,128]{1,0:T(8,128)(2,1)} %collective-permute-done.5), channel_id=1, source_target_pairs={{0,2},{2,0},{4,6},{6,4},{8,10},{10,8},{12,14},{14,12},{16,18},{18,... | collective-permute-start | bytes 1572872 | tf_op jit(solution)/shard_map/ppermute | solution.py:117
  93.8 65.9 %collective-permute-start.13 = (bf16[2048,128]{1,0:T(8,128)(2,1)}, bf16[2048,128]{1,0:T(8,128)(2,1)}, u32[]{:S(2)}, u32[]{:S(2)}) collective-permute-start(bf16[2048,128]{1,0:T(8,128)(2,1)} %collective-permute-done.5), channel_id=1, source_target_pairs={{0,4},{2,6},{4,0},{6,2},{8,12},{10,14},{12,8},{14,10},{16,20},{18,... | collective-permute-start | bytes 1572872 | tf_op jit(solution)/shard_map/ppermute | solution.py:110
  94.3 61.0 %collective-permute-start.8 = (bf16[2048,128]{1,0:T(8,128)(2,1)}, bf16[2048,128]{1,0:T(8,128)(2,1)}, u32[]{:S(2)}, u32[]{:S(2)}) collective-permute-start(bf16[2048,128]{1,0:T(8,128)(2,1)} %collective-permute-done.7), channel_id=1, source_target_pairs={{0,2},{2,0},{4,6},{6,4},{8,10},{10,8},{12,14},{14,12},{16,18},{18,... | collective-permute-start | bytes 1572872 | tf_op jit(solution)/shard_map/ppermute | solution.py:117
  98.3 6.0 %copy-start.11 = (f32[2048]{0:T(1024)S(1)}, f32[2048]{0:T(1024)}, u32[]{:S(2)}) copy-start(f32[2048]{0:T(1024)} %param.16) | copy-start | bytes 24580
  104.9 180.5 %copy-start = (bf16[512,2048]{1,0:T(8,128)(2,1)}, bf16[512,2048]{1,0:T(8,128)(2,1)S(1)}, u32[]{:S(2)}) copy-start(bf16[512,2048]{1,0:T(8,128)(2,1)S(1)} %multiply_convert_fusion.2.stream_ref) | copy-start | bytes 6291460
  124.3 43.8 %collective-permute-start.15 = (bf16[2048,128]{1,0:T(8,128)(2,1)}, bf16[2048,128]{1,0:T(8,128)(2,1)S(1)}, u32[]{:S(2)}, u32[]{:S(2)}) collective-permute-start(bf16[2048,128]{1,0:T(8,128)(2,1)} %collective-permute-done.7), channel_id=1, source_target_pairs={{0,4},{2,6},{4,0},{6,2},{8,12},{10,14},{12,8},{14,10},{16,20},{18,... | collective-permute-start | bytes 1572872 | tf_op jit(solution)/shard_map/ppermute | solution.py:110
  145.4 12.8 %collective-permute-start.10 = (bf16[2048,128]{1,0:T(8,128)(2,1)S(1)}, bf16[2048,128]{1,0:T(8,128)(2,1)S(1)}, u32[]{:S(2)}, u32[]{:S(2)}) collective-permute-start(bf16[2048,128]{1,0:T(8,128)(2,1)S(1)} %collective-permute-done.9), channel_id=1, source_target_pairs={{0,2},{2,0},{4,6},{6,4},{8,10},{10,8},{12,14},{14,12},{16,18},{18,... | collective-permute-start | bytes 1572872 | tf_op jit(solution)/shard_map/ppermute | solution.py:117
  153.1 27.5 %collective-permute-start.17 = (bf16[2048,128]{1,0:T(8,128)(2,1)S(1)}, bf16[2048,128]{1,0:T(8,128)(2,1)S(1)}, u32[]{:S(2)}, u32[]{:S(2)}) collective-permute-start(bf16[2048,128]{1,0:T(8,128)(2,1)S(1)} %collective-permute-done.9), channel_id=1, source_target_pairs={{0,4},{2,6},{4,0},{6,2},{8,12},{10,14},{12,8},{14,10},{16,20},{18,... | collective-permute-start | bytes 1572872 | tf_op jit(solution)/shard_map/ppermute | solution.py:110
  155.4 29.0 %collective-permute-start.12 = (bf16[2048,128]{1,0:T(8,128)(2,1)S(1)}, bf16[2048,128]{1,0:T(8,128)(2,1)S(1)}, u32[]{:S(2)}, u32[]{:S(2)}) collective-permute-start(bf16[2048,128]{1,0:T(8,128)(2,1)S(1)} %collective-permute-done.11), channel_id=1, source_target_pairs={{0,2},{2,0},{4,6},{6,4},{8,10},{10,8},{12,14},{14,12},{16,18},{18,... | collective-permute-start | bytes 1572872 | tf_op jit(solution)/shard_map/ppermute | solution.py:117
  158.2 48.1 %collective-permute-start.19 = (bf16[512,2048]{1,0:T(8,128)(2,1)S(1)}, bf16[512,2048]{1,0:T(8,128)(2,1)}, u32[]{:S(2)}, u32[]{:S(2)}) collective-permute-start(bf16[512,2048]{1,0:T(8,128)(2,1)S(1)} %multiply_convert_fusion.2.stream_ref), channel_id=1, source_target_pairs={{0,1},{1,0},{2,3},{3,2},{4,5},{5,4},{6,7},{7,6},{8,9},{9,8},{10,11... | collective-permute-start | bytes 6291464 | tf_op jit(solution)/shard_map/ppermute | solution.py:93
  159.7 27.6 %collective-permute-start.14 = (bf16[2048,128]{1,0:T(8,128)(2,1)}, bf16[2048,128]{1,0:T(8,128)(2,1)S(1)}, u32[]{:S(2)}, u32[]{:S(2)}) collective-permute-start(bf16[2048,128]{1,0:T(8,128)(2,1)} %collective-permute-done.13), channel_id=1, source_target_pairs={{0,2},{2,0},{4,6},{6,4},{8,10},{10,8},{12,14},{14,12},{16,18},{18,... | collective-permute-start | bytes 1572872 | tf_op jit(solution)/shard_map/ppermute | solution.py:117
  168.0 21.1 %collective-permute-start.16 = (bf16[2048,128]{1,0:T(8,128)(2,1)S(1)}, bf16[2048,128]{1,0:T(8,128)(2,1)S(1)}, u32[]{:S(2)}, u32[]{:S(2)}) collective-permute-start(bf16[2048,128]{1,0:T(8,128)(2,1)S(1)} %collective-permute-done.15), channel_id=1, source_target_pairs={{0,2},{2,0},{4,6},{6,4},{8,10},{10,8},{12,14},{14,12},{16,18},{18,... | collective-permute-start | bytes 1572872 | tf_op jit(solution)/shard_map/ppermute | solution.py:117
  180.6 10.3 %collective-permute-start.18 = (bf16[2048,128]{1,0:T(8,128)(2,1)S(1)}, bf16[2048,128]{1,0:T(8,128)(2,1)S(1)}, u32[]{:S(2)}, u32[]{:S(2)}) collective-permute-start(bf16[2048,128]{1,0:T(8,128)(2,1)S(1)} %collective-permute-done.17), channel_id=1, source_target_pairs={{0,2},{2,0},{4,6},{6,4},{8,10},{10,8},{12,14},{14,12},{16,18},{18,... | collective-permute-start | bytes 1572872 | tf_op jit(solution)/shard_map/ppermute | solution.py:117
  219.4 2.0 copy-start.13
  275.2 7.7 %copy-start.1 = (f32[512,2048]{1,0:T(8,128)S(1)}, f32[512,2048]{1,0:T(8,128)}, u32[]{:S(2)}) copy-start(f32[512,2048]{1,0:T(8,128)} %fusion.5) | copy-start | bytes 12582916
  282.9 22.1 %slice-start = ((s8[8388608]{0:T(1024)(128)(4,1)}), s8[4194304]{0:T(1024)(128)(4,1)S(1)}, s32[]{:S(2)}) async-start(s8[8388608]{0:T(1024)(128)(4,1)} %bitcast.65), calls=%async_computation.3 | async-start | bytes 8388608
  283.9 21.1 %slice-start.1 = ((s8[8388608]{0:T(1024)(128)(4,1)}), s8[4194304]{0:T(1024)(128)(4,1)S(1)}, s32[]{:S(2)}) async-start(s8[8388608]{0:T(1024)(128)(4,1)} %bitcast.65), calls=%async_computation.4 | async-start | bytes 8388608
  283.9 47.8 %collective-permute-start.20 = (bf16[512,2048]{1,0:T(8,128)(2,1)S(1)}, bf16[512,2048]{1,0:T(8,128)(2,1)S(1)}, u32[]{:S(2)}, u32[]{:S(2)}) collective-permute-start(bf16[512,2048]{1,0:T(8,128)(2,1)S(1)} %add_convert_fusion), channel_id=1, source_target_pairs={{0,1},{1,0},{2,3},{3,2},{4,5},{5,4},{6,7},{7,6},{8,9},{9,8},{10,11... | collective-permute-start | bytes 6291464 | tf_op jit(solution)/shard_map/ppermute | solution.py:93
  331.7 1.3 copy-start.5
Sparse Core Ops, SparseCore 0:
  9.5 184.3 all-gather.2
  196.1 79.0 all-gather.4
